TPU v7x, 32 devices: a whole 2x2x4 slice. The times are simulated.
32 devices in a mesh: ep: 8 (over z, x), tp: 4 (over y, core).
Axes of the slice: x: 2, y: 2, z: 4, core: 2. Of those that a mesh axis runs over, the one named last changes fastest.
Arguments:
- queries: bfloat16 [4096, 8, 96], P('ep', 'tp'), may hold values from -240 to 240
- kv_latent: bfloat16 [4096, 128], P(('ep', 'tp')), may hold values from -6 to 6
- rope_key: bfloat16 [4096, 32], P(('ep', 'tp')), may hold values from -6 to 6
- kv_gain: float32 [128], replicated, may hold values from 0.1 to 1.9
- kv_up: bfloat16 [128, 8, 128], P(None, 'tp'), may hold values from -0.5 to 0.5
- mix_out: bfloat16 [8, 64, 2048], P('tp'), may hold values from -0.25 to 0.25
- moe_in: bfloat16 [2048, 2048], P('ep', 'tp'), may hold values from -6 to 6
- moe_gain: float32 [2048], replicated, may hold values from 0.1 to 1.9
- routes: int32 [2048, 2], P('ep'), may hold values from 0 to 7, all different within a row; in each aligned block of 256 rows (0 to 255, 256 to 511, ...) at most 68 rows name the same one
- route_weights: float32 [2048, 2], P('ep'), may hold values from 0.1 to 1
- gate_w: bfloat16 [8, 2048, 3584], P('ep', None, 'tp'), may hold values from -0.125 to 0.125
- up_w: bfloat16 [8, 2048, 3584], P('ep', None, 'tp'), may hold values from -0.125 to 0.125
- down_w: bfloat16 [8, 3584, 2048], P('ep', 'tp'), may hold values from -0.09375 to 0.09375
Outputs:
- mixed: bfloat16 [4096, 2048], P(('ep', 'tp'))
- moe_out: bfloat16 [2048, 2048], P('ep', 'tp')
Inputs may be any that keep to these rules, and one draw needn't show every extreme that they name: `routes`: among the rows of one index of ep, no expert is named by more than 68 entries, a bound that some block reaches; a row names 2 different experts.
All inputs are finite; a program needn't handle non-finite values.
Results may differ from a plain program's by a relative error of at most 0.025.
Values may be sent and summed in bfloat16 or wider, within the bound.
A program may use at most 128 MiB of HBM per device.

v0:
```python
import math
import jax
import jax.numpy as jnp
from jax import lax
from jax.sharding import PartitionSpec as P

D = 2048
NOPE = 64
SEQS = 1
eps = 1e-06
rope_base = 10000.0
neg_big = -1e30


def rotate(values, positions):
    half_dim = values.shape[-1] // 2
    inv_freq = rope_base ** (-jnp.arange(half_dim, dtype=jnp.float32) * 2.0 / values.shape[-1])
    angles = positions.astype(jnp.float32)[:, None] * inv_freq[None, :]
    angles = angles.reshape((angles.shape[0],) + (1,) * (values.ndim - 2) + (half_dim,))
    cosine = jnp.cos(angles)
    sine_part = jnp.sin(angles)
    first_half = values[..., :half_dim].astype(jnp.float32)
    second_half = values[..., half_dim:].astype(jnp.float32)
    return jnp.concatenate(
        [
            first_half * cosine - second_half * sine_part,
            second_half * cosine + first_half * sine_part,
        ],
        axis=-1,
    )


def shards(
    queries,
    kv_latent,
    rope_key,
    kv_gain,
    kv_up,
    mix_out,
    moe_in,
    moe_gain,
    routes,
    route_weights,
    gate_w,
    up_w,
    down_w,
):
    block_rows = queries.shape[0]
    heads_here = queries.shape[1]
    value_dim = kv_up.shape[-1] - NOPE
    seq_len = block_rows * lax.axis_size("ep") // SEQS
    query_start = lax.axis_index("ep") * block_rows
    query_index = query_start + jnp.arange(block_rows, dtype=jnp.int32)
    seq_start = query_start // seq_len * seq_len
    query_nope = queries[..., :NOPE]
    query_rot = rotate(queries[..., NOPE:], query_index % seq_len).astype(jnp.bfloat16)
    score_scale = 1.0 / math.sqrt(queries.shape[-1])
    initial = (
        jnp.full((block_rows, heads_here), neg_big, jnp.float32),
        jnp.zeros((block_rows, heads_here), jnp.float32),
        jnp.zeros((block_rows, heads_here, value_dim), jnp.float32),
    )
    latent_piece = lax.all_gather(kv_latent, ("ep", "tp"), axis=0, tiled=True)
    rope_piece = lax.all_gather(rope_key, ("ep", "tp"), axis=0, tiled=True)
    piece_rows = latent_piece.shape[0]
    sub_rows = math.gcd(piece_rows, 512)

    def sub_block(state_in, offset):

        def attend_piece(state_run):
            running_max, running_sum, weighted = state_run
            latent_rows = lax.dynamic_slice_in_dim(latent_piece, offset, sub_rows, 0).astype(
                jnp.float32
            )
            rope_rows = lax.dynamic_slice_in_dim(rope_piece, offset, sub_rows, 0)
            key_ids = offset + jnp.arange(sub_rows, dtype=jnp.int32)
            normed = (
                latent_rows
                * lax.rsqrt(jnp.mean(latent_rows * latent_rows, axis=-1, keepdims=True) + eps)
                * kv_gain
            ).astype(jnp.bfloat16)
            head_proj = jnp.einsum(
                "nr,rhd->nhd", normed, kv_up, preferred_element_type=jnp.float32
            ).astype(jnp.bfloat16)
            key_rot = rotate(rope_rows, key_ids % seq_len).astype(jnp.bfloat16)
            scores = jnp.einsum(
                "qhd,khd->qhk",
                query_nope,
                head_proj[..., :NOPE],
                preferred_element_type=jnp.float32,
            )
            scores = (
                scores
                + jnp.einsum("qhd,kd->qhk", query_rot, key_rot, preferred_element_type=jnp.float32)
            ) * score_scale
            allowed = (
                (key_ids[None, :] <= query_index[:, None]) & (key_ids[None, :] >= seq_start)
            )[:, None, :]
            scores = jnp.where(allowed, scores, neg_big)
            new_max = jnp.maximum(running_max, jnp.max(scores, axis=-1))
            exp_scores = jnp.where(allowed, jnp.exp(scores - new_max[..., None]), 0.0)
            rescale = jnp.exp(running_max - new_max)
            running_sum = running_sum * rescale + jnp.sum(exp_scores, axis=-1)
            weighted = weighted * rescale[..., None] + jnp.einsum(
                "qhk,khd->qhd",
                exp_scores.astype(jnp.bfloat16),
                head_proj[..., NOPE:],
                preferred_element_type=jnp.float32,
            )
            return (new_max, running_sum, weighted)

        is_needed = (offset < query_start + block_rows) & (offset + sub_rows > seq_start)
        return (lax.cond(is_needed, attend_piece, lambda state_run: state_run, state_in), None)

    state_out, _ = lax.scan(
        sub_block, initial, jnp.arange(0, piece_rows, sub_rows, dtype=jnp.int32)
    )
    running_max, running_sum, weighted = state_out
    attn = (weighted / running_sum[..., None]).astype(jnp.bfloat16)
    mixed = lax.psum_scatter(
        jnp.einsum("thv,hvd->td", attn, mix_out, preferred_element_type=jnp.float32).astype(
            jnp.bfloat16
        ),
        "tp",
        scatter_dimension=0,
        tiled=True,
    )
    rows_here = routes.shape[0]
    top_count = routes.shape[1]
    experts = gate_w.shape[0] * lax.axis_size("ep")
    mean_slots = top_count * rows_here // experts
    capacity = mean_slots + max(mean_slots // 16, 1)
    flat_routes = routes.reshape(-1)
    onehot = (flat_routes[:, None] == jnp.arange(experts, dtype=jnp.int32)[None, :]).astype(
        jnp.int32
    )
    slot_rank = jnp.sum((jnp.cumsum(onehot, axis=0) - onehot) * onehot, axis=1)
    slot_dest = flat_routes * capacity + slot_rank
    slot_owner = (
        jnp.full((experts * capacity,), -1, jnp.int32)
        .at[slot_dest]
        .set(jnp.arange(rows_here * top_count, dtype=jnp.int32))
    )
    is_valid = slot_owner >= 0
    token_row = jnp.maximum(slot_owner, 0) // top_count
    send_rows = jnp.where(is_valid[:, None], moe_in[token_row], 0).reshape(
        experts, capacity, moe_in.shape[1]
    )
    arrived = lax.all_to_all(send_rows, "ep", split_axis=0, concat_axis=0, tiled=True)
    piece_f = lax.all_gather(arrived, "tp", axis=2, tiled=True).astype(jnp.float32)
    scaled = (piece_f * moe_gain).astype(jnp.bfloat16)
    gate_rows = gate_w[0]
    up_rows = up_w[0]
    gate_acc = jnp.einsum("scd,df->scf", scaled, gate_rows, preferred_element_type=jnp.float32)
    up_acc = jnp.einsum("scd,df->scf", scaled, up_rows, preferred_element_type=jnp.float32)
    squares = jnp.sum(piece_f * piece_f, axis=-1)
    gate_acc, up_acc, squares = (gate_acc, up_acc, squares)
    row_scale = lax.rsqrt(squares / D + eps)[..., None]
    hidden = (jax.nn.silu(gate_acc * row_scale) * (up_acc * row_scale)).astype(jnp.bfloat16)
    partial_value = jnp.einsum("scf,fd->scd", hidden, down_w[0], preferred_element_type=jnp.float32)
    summed = lax.psum_scatter(
        partial_value.astype(jnp.bfloat16), "tp", scatter_dimension=2, tiled=True
    )
    returned = lax.all_to_all(summed, "ep", split_axis=0, concat_axis=0, tiled=True)
    flat_back = returned.reshape(experts * capacity, returned.shape[-1])
    picked = (
        flat_back[slot_dest].astype(jnp.float32).reshape(rows_here, top_count, returned.shape[-1])
    )
    moe_out = jnp.sum(picked * route_weights[..., None], axis=1).astype(jnp.bfloat16)
    return (mixed, moe_out)


def solution(mesh):
    in_specs = (
        P("ep", "tp", None),
        P(("ep", "tp"), None),
        P(("ep", "tp"), None),
        P(),
        P(None, "tp", None),
        P("tp", None, None),
        P("ep", "tp"),
        P(),
        P("ep", None),
        P("ep", None),
        P("ep", None, "tp"),
        P("ep", None, "tp"),
        P("ep", "tp", None),
    )
    out_specs = (P(("ep", "tp"), None), P("ep", "tp"))
    return jax.shard_map(shards, mesh=mesh, in_specs=in_specs, out_specs=out_specs, check_vma=False)
```

profile of v0, /device:TPU:0, one launch (start us, length us, event | category | flops | bytes accessed | tf_op | source)
XLA Modules:
  0.0 246.8 jit_solution(13989375117769268064)
XLA Ops:
  7.2 0.0 copy-start
  7.2 0.0 all-gather.5.cloned.1.call-start
  7.2 0.9 copy.21
  8.1 0.1 eq.32
  8.3 0.1 eq.28
  8.4 0.7 broadcast_multiply_fusion
  9.1 1.1 reduce-window.6
  10.2 0.2 slice_reduce_fusion
  10.5 0.1 copy.20
  10.6 0.1 mul.192
  10.8 0.1 fusion.67
  10.9 2.4 scatter_custom_fusion
  13.4 2.7 %gather_fusion = bf16[544,512]{1,0:T(8,128)(2,1)S(1)} fusion(bf16[256,512]{1,0:T(8,128)(2,1)S(1)} %copy-done.1, s32[1024]{0:T(1024)S(1)} %pad_clamp_fusion.1), kind=kCustom, calls=%fused_computation | custom fusion | bytes 1116288 | tf_op jit(solution)/shard_map/gather | solution.py:146
  16.1 0.1 gather.9
  16.3 0.1 broadcast_in_dim.71
  16.3 0.1 broadcast_select_fusion
  16.5 0.0 copy-start.8
  16.5 23.7 %all_to_all.10 = bf16[8,68,512]{2,1,0:T(8,128)(2,1)} all-to-all(bf16[8,68,512]{2,1,0:T(8,128)(2,1)S(1)} %broadcast_select_fusion), channel_id=1, replica_groups=mesh['ep'=8,'tp'=4] {'ep'}, dimensions={0} | all-to-all | bytes 1114112 | tf_op jit(solution)/shard_map/all_to_all | solution.py:149
  40.2 0.0 all-gather.5.cloned.1.call-update
  40.2 0.0 all-gather.3.cloned.1.call-start
  40.3 0.7 all-gather.3.cloned.1.call-update
  41.0 0.0 reduce-scatter.5.cloned.1.call-start
  41.0 21.8 %all-gather.5.cloned.1.call-done = bf16[8,68,2048]{2,1,0:T(8,128)(2,1)} async-done(((bf16[8,68,512]{2,1,0:T(8,128)(2,1)}), bf16[8,68,2048]{2,1,0:T(8,128)(2,1)}) %all-gather.5.cloned.1.call-update) | async-done | bytes 2228240 | tf_op jit(solution)/shard_map/all_gather | solution.py:150
  62.9 2.4 fusion.39
  65.3 6.0 %fusion.42 = f32[8,68,896]{2,1,0:T(8,128)} fusion(bf16[1,2048,896]{2,1,0:T(8,128)(2,1)} %param.28, bf16[8,68,2048]{2,1,0:T(8,128)(2,1)S(1)} %copy-done.2, f32[2048]{0:T(1024)S(1)} %copy-done.8), kind=kOutput, calls=%fused_computation.63 | convolution fusion | flops 1999831040 | bytes 7856128 | tf_op jit(solution)/shard_map/scd,df->scf/dot_general | solution.py:155
  71.3 10.5 %fusion.46 = bf16[8,68,2048]{2,1,0:T(8,128)(2,1)} fusion(bf16[1,896,2048]{2,1,0:T(8,128)(2,1)} %param.29, f32[8,68,896]{2,1,0:T(8,128)} %fusion.42, bf16[1,2048,896]{2,1,0:T(8,128)(2,1)} %param.27, bf16[8,68,2048]{2,1,0:T(8,128)(2,1)S(1)} %copy-done.2, f32[2048]{0:T(1024)S(1)} %copy-done.8, f32[8,68]{1,0:T(8,128)S(1)} %add_rsqrt_fusion.1), kind=kOutput, calls=%fused_computation.67 | convolution fusion | flops 4001333248 | bytes 13756544 | tf_op jit(solution)/shard_map/scf,fd->scd/dot_general | solution.py:160
  81.8 0.0 reduce-scatter.5.cloned.1.call-update
  81.8 0.0 reduce-scatter.3.cloned.1.call-start
  81.9 0.8 copy-done.3
  82.7 0.1 copy.19
  82.9 0.2 multiply_cosine_fusion.1
  83.2 44.1 %all_gather.10 = bf16[4096,32]{0,1:T(8,128)(2,1)} all-gather(bf16[128,32]{0,1:T(8,128)(2,1)S(1)} %copy-done.6), channel_id=1, replica_groups=mesh['ep'=8,'tp'=4] {'ep','tp'}, dimensions={0}, use_global_device_ids=true | all-gather | bytes 270336 | tf_op jit(solution)/shard_map/all_gather | solution.py:64
  127.3 0.0 copy-done.5
  127.3 22.8 %while.17 = (s32[]{:T(128)}, f32[512,2]{0,1:T(2,128)S(1)}, f32[512,2]{0,1:T(2,128)S(1)}, f32[512,2,64]{0,2,1:T(8,128)S(1)}, s32[8]{0:T(128)S(1)}, /*index=5*/s32...) while((s32[]{:T(128)}, f32[512,2]{0,1:T(2,128)S(1)}, ...), condition=%wide.region_6.7_spmd.clone, body=%wide.region_0.6_spmd.clone.sunk | while | flops 207981088 | bytes 14346293 | solution.py:115
  127.3 0.6 dynamic_slice.19
  129.0 8.8 %conditional.3 = ((f32[512,2]{0,1:T(2,128)S(1)}, f32[512,2]{0,1:T(2,128)S(1)}, f32[512,2,64]{0,2,1:T(8,128)S(1)})) conditional(s32[]{:T(128)} %convert_element_type.174, (f32[512,2]{0,1:T(2,128)S(1)}, f32[512,2]{0,1:T(2,128)S(1)}, f32[512,2,64]{0,2,1:T(8,128)S(1)}) %tuple.51, (s32[]{:T(128)}, s32[]{:T(128)}, s32[]{:T(128)}, ...), branch_computations={%region_1.1_spmd, %region_2.5_spmd} | conditional | flops 207981088 | bytes 14343918 | solution.py:113
  130.7 1.1 fusion.11
  131.8 1.2 fusion.14
  133.1 0.5 fusion.17
  133.6 0.6 fusion.33
  134.2 1.0 fusion.27
  135.1 0.6 fusion.34
  135.7 0.2 compare_and_fusion
  136.0 0.7 fusion.75
  136.7 0.4 fusion.5
  137.2 0.7 fusion.6
  137.8 0.6 dynamic_slice.19
  139.6 0.6 dynamic_slice.19
  141.4 0.6 dynamic_slice.19
  143.1 0.6 dynamic_slice.19
  144.9 0.6 dynamic_slice.19
  146.6 0.6 dynamic_slice.19
  148.4 0.6 dynamic_slice.19
  150.2 2.1 bitcast_convert_fusion
  152.2 0.0 reduce-scatter.3.cloned.1.call-update
  152.2 1.7 reduce-scatter.5.cloned.1.call-done
  153.9 59.0 %all-to-all-start.1 = ((bf16[8,68,512]{2,1,0:T(8,128)(2,1)}), bf16[8,68,512]{2,1,0:T(8,128)(2,1)S(1)}, u32[]{:S(2)}, u32[]{:S(2)}) async-start(bf16[8,68,512]{2,1,0:T(8,128)(2,1)} %reduce-scatter.5.cloned.1.call-done), calls=%async_computation.3 | async-start | bytes 1179648 | tf_op jit(solution)/shard_map/all_to_all | solution.py:164
  212.9 0.1 copy.23
  213.1 16.2 %all-to-all-done.1 = bf16[8,68,512]{2,1,0:T(8,128)(2,1)S(1)} async-done(((bf16[8,68,512]{2,1,0:T(8,128)(2,1)}), bf16[8,68,512]{2,1,0:T(8,128)(2,1)S(1)}, u32[]{:S(2)}, u32[]{:S(2)}) %all-to-all-start.1) | async-done | bytes 557088 | tf_op jit(solution)/shard_map/all_to_all | solution.py:164
  229.3 0.1 reshape.222
  229.4 2.0 gather_fusion.1
  231.4 0.7 reshape.223
  232.1 2.1 multiply_reduce_fusion
  234.1 6.1 %reduce-scatter.3.cloned.1.call-done = bf16[128,2048]{1,0:T(8,128)(2,1)} async-done(((bf16[512,2048]{1,0:T(8,128)(2,1)}), bf16[128,2048]{1,0:T(8,128)(2,1)}) %reduce-scatter.3.cloned.1.call-update) | async-done | bytes 524304 | tf_op jit(solution)/shard_map/reduce_scatter | solution.py:120
  (56 shorter events, 0.4 us)
Async XLA Ops:
  7.2 143.0 %copy-start = (bf16[2,64,2048]{2,1,0:T(8,128)(2,1)S(1)}, bf16[2,64,2048]{2,1,0:T(8,128)(2,1)}, u32[]{:S(2)}) copy-start(bf16[2,64,2048]{2,1,0:T(8,128)(2,1)} %param.22) | copy-start | bytes 1572868
  7.2 6.2 %copy-start.1 = (bf16[256,512]{1,0:T(8,128)(2,1)S(1)}, bf16[256,512]{1,0:T(8,128)(2,1)}, u32[]{:S(2)}) copy-start(bf16[256,512]{1,0:T(8,128)(2,1)} %param.23) | copy-start | bytes 786436
  7.2 55.7 %all-gather.5.cloned.1.call-start = ((), (), s32[]{:S(2)}) async-start(), calls=%async_computation.6 | async-start | bytes 2949120 | tf_op jit(solution)/shard_map/all_gather | solution.py:150
  16.5 48.8 %copy-start.8 = (f32[2048]{0:T(1024)S(1)}, f32[2048]{0:T(1024)}, u32[]{:S(2)}) copy-start(f32[2048]{0:T(1024)} %param.24) | copy-start | bytes 24580
  40.2 87.0 %all-gather.3.cloned.1.call-start = ((), (), s32[]{:S(2)}) async-start(), calls=%async_computation.4 | async-start | bytes 1081344 | tf_op jit(solution)/shard_map/all_gather | solution.py:63
  41.0 112.9 %reduce-scatter.5.cloned.1.call-start = ((), (), s32[]{:S(2)}) async-start(), calls=%async_computation.7 | async-start | bytes 2949120 | tf_op jit(solution)/shard_map/reduce_scatter | solution.py:161
  62.9 2.4 copy-start.2
  81.8 0.9 copy-start.3
  81.8 0.9 copy-start.4
  81.8 1.4 copy-start.6
  81.8 45.5 %copy-start.5 = (f32[128]{0:T(128)S(1)}, f32[128]{0:T(128)}, u32[]{:S(2)}) copy-start(f32[128]{0:T(128)} %param.20) | copy-start | bytes 1540
  81.8 158.5 %reduce-scatter.3.cloned.1.call-start = ((), (), s32[]{:S(2)}) async-start(), calls=%async_computation.5 | async-start | bytes 2621440 | tf_op jit(solution)/shard_map/reduce_scatter | solution.py:120
  152.2 60.7 %copy-start.7 = (f32[256,2]{0,1:T(2,128)S(1)}, f32[256,2]{0,1:T(2,128)}, u32[]{:S(2)}) copy-start(f32[256,2]{0,1:T(2,128)} %param.26) | copy-start | bytes 6148
  153.9 75.4 %all-to-all-start.1 = ((bf16[8,68,512]{2,1,0:T(8,128)(2,1)}), bf16[8,68,512]{2,1,0:T(8,128)(2,1)S(1)}, u32[]{:S(2)}, u32[]{:S(2)}) async-start(bf16[8,68,512]{2,1,0:T(8,128)(2,1)} %reduce-scatter.5.cloned.1.call-done), calls=%async_computation.3 | async-start | bytes 1179648 | tf_op jit(solution)/shard_map/all_to_all | solution.py:164
Sparse Core Ops, SparseCore 0:
  40.4 22.4 all-gather.4
  65.8 53.8 all-gather.2
  122.2 31.7 reduce-scatter.4
  156.9 83.3 reduce-scatter.2
where the time goes:
time: 248 us; the launch traced here: 247 us
  blocking collectives  67.8 us (27%)
  starting transfers between devices  59.1 us (24%)
  waiting for transfers between devices  46.7 us (19%)
  matrix products  21.6 us (9%)
  local copies, waits for them, and re-layouts  15.6 us (6%)
  between operations  14.1 us (6%)
  loops' own time  11.2 us (5%)
  other arithmetic  10.8 us (4%)
    all_to_all x1, starting transfers between devices, shards(): lax.all_to_all(summed, 'ep', split_axis=0, concat_axis=0, tiled=True)  59 us
    all_gather x1, blocking collectives, shards(): rope_piece = lax.all_gather(rope_key, ('ep', 'tp'), axis=0, tiled=True)  44.1 us
    all_to_all x1, blocking collectives, shards(): lax.all_to_all(send_rows, 'ep', split_axis=0, concat_axis=0, tiled=True)  23.7 us
    all_gather x1, waiting for transfers between devices, shards(): lax.all_gather(arrived, 'tp', axis=2, tiled=True).astype(jnp.float32)  21.8 us
    all_to_all x1, waiting for transfers between devices, shards(): lax.all_to_all(summed, 'ep', split_axis=0, concat_axis=0, tiled=True)  16.2 us
    dot_general x1, matrix products, shards(): jnp.einsum('scf,fd->scd', hidden, down_w[0], preferred_element_type=jnp.f...  10.5 us
    another operation x1, loops' own time, shards(): lax.scan(sub_block, initial, jnp.arange(0, piece_rows, sub_rows, dtype=jn...  9.28 us
    reduce_scatter x1, waiting for transfers between devices, shards(): lax.psum_scatter(jnp.einsum('thv,hvd->td', attn, mix_out, preferred_eleme...  6.14 us
  transfers between devices with their start and end apart: 5, of which 4 were waited for; matrix products, arithmetic and copies ran while one was open for 15% of the time, Pallas kernels for 0%

commit v1 on v0

--- a/solution.py
+++ b/solution.py
@@ -147,7 +147,7 @@
         experts, capacity, moe_in.shape[1]
     )
     arrived = lax.all_to_all(send_rows, "ep", split_axis=0, concat_axis=0, tiled=True)
-    piece_f = lax.all_gather(arrived, "tp", axis=2, tiled=True).astype(jnp.float32)
+    piece_f = jnp.concatenate(lax.all_gather(arrived, "tp"), axis=2).astype(jnp.float32)
     scaled = (piece_f * moe_gain).astype(jnp.bfloat16)
     gate_rows = gate_w[0]
     up_rows = up_w[0]

time: 248 us -> 257 us (1.036)
  local copies, waits for them, and re-layouts: 15.6 us -> 20.1 us
  other arithmetic: 10.8 us -> 15.1 us
  blocking collectives: 67.8 us -> 65.1 us
    convert_element_type x0 -> x2, other arithmetic: none -> 4.85 us  [the longest x1 4.24 us: shards(): scaled = (piece_f * moe_gain).astype(jnp.bfloat16)]
    convert_element_type x0 -> x1, local copies, waits for them, and re-layouts: none -> 3 us  [shards(): scaled = (piece_f * moe_gain).astype(jnp.bfloat16)]
    all_gather x1, blocking collectives: 44.1 us -> 41.4 us  [shards(): rope_piece = lax.all_gather(rope_key, ('ep', 'tp'), axis=0, tiled=True)]
  transfers between devices with their start and end apart: 5 -> 5, of which waited for: 4 -> 3; matrix products, arithmetic and copies ran while one was open for 15% -> 19% of each run, Pallas kernels for 0% -> 0%
where the time goes in v1:
time: 257 us; the launch traced here: 255 us
  blocking collectives  65.1 us (25%)
  starting transfers between devices  59.9 us (23%)
  waiting for transfers between devices  44.2 us (17%)
  matrix products  23.4 us (9%)
  local copies, waits for them, and re-layouts  20.1 us (8%)
  other arithmetic  15.1 us (6%)
  between operations  14.1 us (5%)
  loops' own time  13.7 us (5%)
    all_to_all x1, starting transfers between devices, shards(): lax.all_to_all(summed, 'ep', split_axis=0, concat_axis=0, tiled=True)  59.7 us
    all_gather x1, blocking collectives, shards(): rope_piece = lax.all_gather(rope_key, ('ep', 'tp'), axis=0, tiled=True)  41.4 us
    all_to_all x1, blocking collectives, shards(): lax.all_to_all(send_rows, 'ep', split_axis=0, concat_axis=0, tiled=True)  23.6 us
    all_gather x1, waiting for transfers between devices, shards(): lax.all_gather(arrived, 'tp')  21.1 us
    all_to_all x1, waiting for transfers between devices, shards(): lax.all_to_all(summed, 'ep', split_axis=0, concat_axis=0, tiled=True)  16.2 us
    another operation x1, loops' own time, shards(): lax.scan(sub_block, initial, jnp.arange(0, piece_rows, sub_rows, dtype=jn...  11.4 us
    dot_general x1, matrix products, shards(): jnp.einsum('scf,fd->scd', hidden, down_w[0], preferred_element_type=jnp.f...  11 us
    dot_general x1, matrix products, shards(): jnp.einsum('scd,df->scf', scaled, up_rows, preferred_element_type=jnp.flo...  7.25 us
  transfers between devices with their start and end apart: 5, of which 3 were waited for; matrix products, arithmetic and copies ran while one was open for 19% of the time, Pallas kernels for 0%

profile of v1, /device:TPU:0, one launch (start us, length us, event | category | flops | bytes accessed | tf_op | source)
XLA Modules:
  0.0 255.5 jit_solution(5770789361233274126)
XLA Ops:
  7.2 0.0 all-gather.6.cloned.1.call-start
  7.2 0.8 broadcast_multiply_fusion
  8.0 0.8 copy.51
  8.8 0.1 eq.32
  9.0 0.1 eq.28
  9.1 0.1 copy.50
  9.2 0.1 mul.199
  9.4 1.1 reduce-window.6
  10.6 0.2 slice_reduce_fusion
  10.8 0.1 fusion.67
  10.9 2.4 scatter_custom_fusion
  13.4 0.1 broadcast_in_dim.71
  13.5 2.7 %gather_fusion = bf16[544,512]{1,0:T(8,128)(2,1)S(1)} fusion(bf16[256,512]{1,0:T(8,128)(2,1)S(1)} %copy-done.1, s32[1024]{0:T(1024)S(1)} %pad_clamp_fusion.1), kind=kCustom, calls=%fused_computation | custom fusion | bytes 1116288 | tf_op jit(solution)/shard_map/gather | solution.py:146
  16.3 0.1 gather.9
  16.4 0.1 broadcast_select_fusion
  16.5 23.6 %all_to_all.10 = bf16[8,68,512]{2,1,0:T(8,128)(2,1)S(1)} all-to-all(bf16[8,68,512]{2,1,0:T(8,128)(2,1)S(1)} %broadcast_select_fusion), channel_id=1, replica_groups=mesh['ep'=8,'tp'=4] {'ep'}, dimensions={0} | all-to-all | bytes 1114112 | tf_op jit(solution)/shard_map/all_to_all | solution.py:149
  40.1 1.0 copy.53
  41.1 0.0 all-gather.4.cloned.1.call-start
  41.2 0.7 all-gather.4.cloned.1.call-update
  41.9 0.0 reduce-scatter.5.cloned.1.call-start
  42.0 21.1 %all-gather.6.cloned.1.call-done = bf16[32,68,512]{2,0,1:T(8,128)(2,1)} async-done(((bf16[8,68,512]{2,0,1:T(8,128)(2,1)}), bf16[32,68,512]{2,0,1:T(8,128)(2,1)}) %all-gather.6.cloned.1.call-update) | async-done | bytes 2228240 | tf_op jit(solution)/shard_map/all_gather | solution.py:150
  63.0 2.3 multiply_reduce_fusion
  65.3 0.1 copy.56
  65.4 0.6 bitcast_convert_fusion.1
  66.0 4.2 %fusion.48 = bf16[8,68,4,512]{3,2,0,1:T(4,128)(2,1)S(1)} fusion(f32[4,8,68,512]{3,1,0,2:T(8,128)S(1)} %bitcast_convert_fusion.1, f32[4,512]{1,0:T(4,128)S(1)} %mul.201), kind=kLoop, calls=%fused_computation.67 | loop fusion | flops 2228224 | bytes 6692864 | tf_op jit(solution)/shard_map/convert_element_type | solution.py:151
  70.3 3.0 %convert_element_type.103 = bf16[8,68,2048]{2,0,1:T(8,128)(2,1)} reshape(bf16[8,68,4,512]{3,2,0,1:T(4,128)(2,1)S(1)} %fusion.48) | data formatting | bytes 4456448 | tf_op jit(solution)/shard_map/convert_element_type | solution.py:151
  73.3 7.3 %fusion.41 = f32[8,68,896]{2,1,0:T(8,128)} fusion(bf16[1,2048,896]{2,1,0:T(8,128)(2,1)} %param.28, bf16[8,68,2048]{2,0,1:T(8,128)(2,1)} %convert_element_type.103), kind=kOutput, calls=%fused_computation.62 | convolution fusion | flops 1996488704 | bytes 7847936 | tf_op jit(solution)/shard_map/scd,df->scf/dot_general | solution.py:155
  80.5 11.0 %fusion.45 = bf16[8,68,2048]{2,1,0:T(8,128)(2,1)} fusion(bf16[1,896,2048]{2,1,0:T(8,128)(2,1)} %param.29, f32[8,68,896]{2,1,0:T(8,128)} %fusion.41, bf16[1,2048,896]{2,1,0:T(8,128)(2,1)} %param.27, bf16[8,68,2048]{2,0,1:T(8,128)(2,1)S(1)} %copy-done.3, f32[8,68]{1,0:T(8,128)S(1)} %add_rsqrt_fusion.1), kind=kOutput, calls=%fused_computation.66 | convolution fusion | flops 3997990912 | bytes 13748352 | tf_op jit(solution)/shard_map/scf,fd->scd/dot_general | solution.py:160
  91.5 0.0 reduce-scatter.5.cloned.1.call-update
  91.5 0.0 reduce-scatter.3.cloned.1.call-start
  91.6 0.7 copy-done.5
  92.3 0.1 copy.49
  92.5 0.2 multiply_cosine_fusion.1
  92.8 41.4 %all_gather.13 = bf16[4096,32]{0,1:T(8,128)(2,1)S(1)} all-gather(bf16[128,32]{0,1:T(8,128)(2,1)S(1)} %copy-done.7), channel_id=1, replica_groups=mesh['ep'=8,'tp'=4] {'ep','tp'}, dimensions={0}, use_global_device_ids=true | all-gather | bytes 270336 | tf_op jit(solution)/shard_map/all_gather | solution.py:64
  134.3 25.5 %while.17 = (s32[]{:T(128)}, f32[512,2]{0,1:T(2,128)S(1)}, f32[512,2]{0,1:T(2,128)S(1)}, f32[512,2,64]{0,2,1:T(8,128)S(1)}, s32[8]{0:T(128)S(1)}, /*index=5*/s32...) while((s32[]{:T(128)}, f32[512,2]{0,1:T(2,128)S(1)}, ...), condition=%wide.region_6.7_spmd.clone, body=%wide.region_0.6_spmd.clone.sunk | while | flops 207981088 | bytes 14346301 | solution.py:115
  134.3 0.7 dynamic_slice.19
  136.4 8.7 %conditional.3 = ((f32[512,2]{0,1:T(2,128)S(1)}, f32[512,2]{0,1:T(2,128)S(1)}, f32[512,2,64]{0,2,1:T(8,128)S(1)})) conditional(s32[]{:T(128)} %convert_element_type.172, (f32[512,2]{0,1:T(2,128)S(1)}, f32[512,2]{0,1:T(2,128)S(1)}, f32[512,2,64]{0,2,1:T(8,128)S(1)}) %tuple.54, (s32[]{:T(128)}, s32[]{:T(128)}, s32[]{:T(128)}, ...), branch_computations={%region_1.1_spmd, %region_2.5_spmd} | conditional | flops 207981088 | bytes 14343918 | solution.py:113
  138.5 0.7 fusion.34
  139.2 1.1 fusion.11
  140.2 1.2 fusion.14
  141.5 0.7 fusion.33
  142.2 0.2 fusion.27
  142.4 0.2 compare_and_fusion
  142.7 0.5 fusion.17
  143.2 0.7 fusion.75
  143.9 0.4 fusion.5
  144.4 0.7 fusion.6
  145.1 0.7 dynamic_slice.19
  147.2 0.7 dynamic_slice.19
  149.3 0.7 dynamic_slice.19
  151.4 0.7 dynamic_slice.19
  153.5 0.7 dynamic_slice.19
  155.6 0.7 dynamic_slice.19
  157.7 0.7 dynamic_slice.19
  159.8 2.1 bitcast_convert_fusion
  161.9 0.0 reduce-scatter.5.cloned.1.call-done
  161.9 59.7 %all-to-all-start.1 = ((bf16[8,68,512]{2,1,0:T(8,128)(2,1)}), bf16[8,68,512]{2,1,0:T(8,128)(2,1)S(1)}, u32[]{:S(2)}, u32[]{:S(2)}) async-start(bf16[8,68,512]{2,1,0:T(8,128)(2,1)} %reduce-scatter.5.cloned.1.call-done), calls=%async_computation.3 | async-start | bytes 1179648 | tf_op jit(solution)/shard_map/all_to_all | solution.py:164
  221.6 0.1 copy.58
  221.8 16.2 %all-to-all-done.1 = bf16[8,68,512]{2,1,0:T(8,128)(2,1)S(1)} async-done(((bf16[8,68,512]{2,1,0:T(8,128)(2,1)}), bf16[8,68,512]{2,1,0:T(8,128)(2,1)S(1)}, u32[]{:S(2)}, u32[]{:S(2)}) %all-to-all-start.1) | async-done | bytes 557088 | tf_op jit(solution)/shard_map/all_to_all | solution.py:164
  238.0 0.1 reshape.229
  238.1 2.0 gather_fusion.1
  240.1 0.7 reshape.230
  240.8 2.1 multiply_reduce_fusion.1
  242.8 6.1 %reduce-scatter.3.cloned.1.call-done = bf16[128,2048]{1,0:T(8,128)(2,1)} async-done(((bf16[512,2048]{1,0:T(8,128)(2,1)}), bf16[128,2048]{1,0:T(8,128)(2,1)}) %reduce-scatter.3.cloned.1.call-update) | async-done | bytes 524304 | tf_op jit(solution)/shard_map/reduce_scatter | solution.py:120
  (64 shorter events, 0.5 us)
Async XLA Ops:
  7.2 152.6 %copy-start = (bf16[2,64,2048]{2,1,0:T(8,128)(2,1)S(1)}, bf16[2,64,2048]{2,1,0:T(8,128)(2,1)}, u32[]{:S(2)}) copy-start(bf16[2,64,2048]{2,1,0:T(8,128)(2,1)} %param.22) | copy-start | bytes 1572868
  7.2 6.3 %copy-start.1 = (bf16[256,512]{1,0:T(8,128)(2,1)S(1)}, bf16[256,512]{1,0:T(8,128)(2,1)}, u32[]{:S(2)}) copy-start(bf16[256,512]{1,0:T(8,128)(2,1)} %param.23) | copy-start | bytes 786436
  7.2 55.9 %all-gather.6.cloned.1.call-start = ((), (), s32[]{:S(2)}) async-start(), calls=%async_computation.7 | async-start | bytes 2785280 | tf_op jit(solution)/shard_map/all_gather | solution.py:150
  16.4 25.6 %copy-start.8 = (f32[2048]{0:T(1024)S(1)}, f32[2048]{0:T(1024)}, u32[]{:S(2)}) copy-start(f32[2048]{0:T(1024)} %param.24) | copy-start | bytes 24580
  41.1 93.1 %all-gather.4.cloned.1.call-start = ((), (), s32[]{:S(2)}) async-start(), calls=%async_computation.4 | async-start | bytes 1081344 | tf_op jit(solution)/shard_map/all_gather | solution.py:63
  41.9 120.0 %reduce-scatter.5.cloned.1.call-start = ((), (), s32[]{:S(2)}) async-start(), calls=%async_computation.6 | async-start | bytes 2949120 | tf_op jit(solution)/shard_map/reduce_scatter | solution.py:161
  63.0 2.4 copy-start.2
  73.3 7.3 %copy-start.3 = (bf16[8,68,2048]{2,0,1:T(8,128)(2,1)S(1)}, bf16[8,68,2048]{2,0,1:T(8,128)(2,1)}, u32[]{:S(2)}) copy-start(bf16[8,68,2048]{2,0,1:T(8,128)(2,1)} %convert_element_type.103) | copy-start | bytes 6684676
  91.5 0.8 copy-start.5
  91.5 1.0 copy-start.4
  91.5 1.3 copy-start.7
  91.5 42.8 %copy-start.6 = (f32[128]{0:T(128)S(1)}, f32[128]{0:T(128)}, u32[]{:S(2)}) copy-start(f32[128]{0:T(128)} %param.20) | copy-start | bytes 1540
  91.5 157.4 %reduce-scatter.3.cloned.1.call-start = ((), (), s32[]{:S(2)}) async-start(), calls=%async_computation.5 | async-start | bytes 2621440 | tf_op jit(solution)/shard_map/reduce_scatter | solution.py:120
  161.9 59.8 %copy-start.9 = (f32[256,2]{0,1:T(2,128)S(1)}, f32[256,2]{0,1:T(2,128)}, u32[]{:S(2)}) copy-start(f32[256,2]{0,1:T(2,128)} %param.26) | copy-start | bytes 6148
  161.9 76.1 %all-to-all-start.1 = ((bf16[8,68,512]{2,1,0:T(8,128)(2,1)}), bf16[8,68,512]{2,1,0:T(8,128)(2,1)S(1)}, u32[]{:S(2)}, u32[]{:S(2)}) async-start(bf16[8,68,512]{2,1,0:T(8,128)(2,1)} %reduce-scatter.5.cloned.1.call-done), calls=%async_computation.3 | async-start | bytes 1179648 | tf_op jit(solution)/shard_map/all_to_all | solution.py:164
Sparse Core Ops, SparseCore 0:
  41.3 21.7 all-gather.5
  65.9 53.9 all-gather.3
  122.4 31.6 reduce-scatter.4
  162.0 86.8 reduce-scatter.2
